TPU v7x, 256 devices: a whole 4x4x8 slice. The times are simulated.
256 devices in a mesh: ep: 64 (over z, x, core), tp: 4 (over y).
Axes of the slice: x: 4, y: 4, z: 8, core: 2. Of those that a mesh axis runs over, the one named last changes fastest.
Arguments:
- residual_in: bfloat16 [1024, 2048], P('ep'), may hold values from -6 to 6
- lengths: int32 [1024], P('ep'), may hold values from 1 to 511, as said below
- kv_cache: bfloat16 [1024, 4, 512, 256], P('ep', 'tp'), may hold values from -640 to 640
- norm_gain_attn: float32 [2048], replicated, may hold values from 0.1 to 1.9
- query_weight: bfloat16 [2048, 2048], P(None, 'tp'), may hold values from -0.125 to 0.125
- key_weight: bfloat16 [2048, 512], P(None, 'tp'), may hold values from -0.125 to 0.125
- value_weight: bfloat16 [2048, 512], P(None, 'tp'), may hold values from -0.125 to 0.125
- diff_lambda: float32 [16], P('tp'), may hold values from 0.3 to 0.8
- head_gain: float32 [128], replicated, may hold values from 0.1 to 1.9
- out_weight: bfloat16 [2048, 2048], P(None, 'tp'), may hold values from -0.125 to 0.125
- norm_gain_ffn: float32 [2048], replicated, may hold values from 0.1 to 1.9
- route_ids: int32 [1024, 2], P('ep'), may hold values from 0 to 63, as said below
- route_weights: float32 [1024, 2], P('ep'), may hold values from 0.1 to 1
- expert_gate: bfloat16 [64, 2048, 512], P('ep', None, 'tp'), may hold values from -0.125 to 0.125
- expert_up: bfloat16 [64, 2048, 512], P('ep', None, 'tp'), may hold values from -0.125 to 0.125
- expert_down: bfloat16 [64, 512, 2048], P('ep', 'tp'), may hold values from -0.25 to 0.25
- dense_gate: bfloat16 [2048, 8192], P(None, 'ep'), may hold values from -0.125 to 0.125
- dense_up: bfloat16 [2048, 8192], P(None, 'ep'), may hold values from -0.125 to 0.125
- dense_down: bfloat16 [8192, 2048], P('ep'), may hold values from -0.0625 to 0.0625
- dense_mix: float32 [2048], replicated, may hold values from -0.125 to 0.125
Outputs:
- layer_out: bfloat16 [1024, 2048], P('ep', 'tp')
- new_rows: bfloat16 [1024, 4, 256], P('ep', 'tp')
Inputs may be any that keep to these rules, and one draw needn't show every extreme that they name: The new token stands at position lengths[b]; some sequence holds 511 positions in every draw. `route_ids`: each row names 2 different experts from one group; the groups are the 4 runs of consecutive expert numbers of equal size. Among the rows of one index of ep no expert is named more than 2 times, and some expert exactly 2 times.
All inputs are finite; a program needn't handle non-finite values.
Results may differ from a plain program's by a relative error of at most 0.008.
The roundings to bfloat16 on the way count: a program that leaves them out, or rounds other values in their place, can miss the bound.
Values may be sent and summed in bfloat16 or wider, within the bound.
A program may use at most 64 MiB of HBM per device.

v0:
```python
import jax
import jax.numpy as jnp
from jax import lax
from jax.sharding import PartitionSpec as P

QK_DIM = 64
HEAD_DIM = 128
TOPK = 2
EPS = 1e-06


def from_everyone(array, axis):
    copies = jnp.broadcast_to(array, (lax.axis_size(axis), *array.shape))
    return lax.all_to_all(copies, axis, split_axis=0, concat_axis=0, tiled=True)


def in_order(pieces, dim):
    pieces = jnp.moveaxis(pieces, 0, dim)
    lengths = pieces.shape
    return pieces.reshape(*lengths[:dim], lengths[dim] * lengths[dim + 1], *lengths[dim + 2 :])


def gather_directly(array, axis, dim):
    pieces = from_everyone(array, axis)
    return in_order(pieces, dim)


def split_up(array, dim, peers):
    lengths = array.shape
    pieces = array.reshape(*lengths[:dim], peers, lengths[dim] // peers, *lengths[dim + 1 :])
    return jnp.moveaxis(pieces, dim, 0)


def summed_on_arrival(array, axis, dim):
    pieces = split_up(array, dim, lax.axis_size(axis))
    arrived = lax.all_to_all(pieces, axis, split_axis=0, concat_axis=0, tiled=True)
    return arrived.astype(jnp.float32).sum(axis=0)


def rms_rows(values, gain):
    mean_sq = jnp.mean(values * values, axis=-1, keepdims=True)
    return values * lax.rsqrt(mean_sq + EPS) * gain


def rotate(vectors, positions):
    half = vectors.shape[-1] // 2
    inverse = 10000.0 ** (-jnp.arange(half, dtype=jnp.float32) / half)
    angle = positions[:, None, None, None] * inverse
    cosine = jnp.cos(angle)
    sine = jnp.sin(angle)
    first = vectors[..., :half]
    second = vectors[..., half:]
    return jnp.concatenate(
        [first * cosine - second * sine, first * sine + second * cosine], axis=-1
    )


def normalize(scores, latest, valid):
    masked = jnp.where(valid, scores, -jnp.inf)
    top = jnp.maximum(jnp.max(masked, axis=-1), latest)
    raised = jnp.where(valid, jnp.exp(jnp.where(valid, scores, 0.0) - top[..., None]), 0.0)
    raised_new = jnp.exp(latest - top)
    total = jnp.sum(raised, axis=-1) + raised_new
    return (raised / total[..., None], raised_new / total)


def attend(query, fresh, cache, lengths, lam):
    count = fresh.shape[0]
    groups = fresh.shape[1]
    share = query.shape[1] // groups
    scale = QK_DIM ** (-0.5)
    grouped = query.reshape(count, groups, share, 2, QK_DIM)
    first = (
        jnp.einsum(
            "bgjd,bgkd->bgjk",
            grouped[:, :, :, 0],
            cache[..., :QK_DIM],
            preferred_element_type=jnp.float32,
        )
        * scale
    )
    second = (
        jnp.einsum(
            "bgjd,bgkd->bgjk",
            grouped[:, :, :, 1],
            cache[..., QK_DIM : 2 * QK_DIM],
            preferred_element_type=jnp.float32,
        )
        * scale
    )
    first_new = (
        jnp.einsum(
            "bgjd,bgd->bgj",
            grouped[:, :, :, 0],
            fresh[..., :QK_DIM],
            preferred_element_type=jnp.float32,
        )
        * scale
    )
    second_new = (
        jnp.einsum(
            "bgjd,bgd->bgj",
            grouped[:, :, :, 1],
            fresh[..., QK_DIM : 2 * QK_DIM],
            preferred_element_type=jnp.float32,
        )
        * scale
    )
    valid = (
        jnp.arange(cache.shape[2], dtype=jnp.int32)[None, None, None, :]
        < lengths[:, None, None, None]
    )
    prob_one, prob_one_new = normalize(first, first_new, valid)
    prob_two, prob_two_new = normalize(second, second_new, valid)
    weight = lam.reshape(groups, share)[None, :, :, None]
    mapped = (prob_one - weight * prob_two).astype(jnp.bfloat16)
    mapped_new = (prob_one_new - weight[..., 0] * prob_two_new).astype(jnp.bfloat16)
    output = jnp.einsum(
        "bgjk,bgkd->bgjd", mapped, cache[..., 2 * QK_DIM :], preferred_element_type=jnp.float32
    )
    output = output + mapped_new.astype(jnp.float32)[..., None] * fresh[
        :, :, None, 2 * QK_DIM :
    ].astype(jnp.float32)
    return output.reshape(count, groups * share, HEAD_DIM)


def on_device(
    residual_in,
    lengths,
    kv_cache,
    norm_gain_attn,
    query_weight,
    key_weight,
    value_weight,
    diff_lambda,
    head_gain,
    out_weight,
    norm_gain_ffn,
    route_ids,
    route_weights,
    expert_gate,
    expert_up,
    expert_down,
    dense_gate,
    dense_up,
    dense_down,
    dense_mix,
):
    seq_count, width = residual_in.shape
    lanes = lax.axis_size("tp")
    column = lax.axis_index("tp")
    quarter = width // lanes
    groups = kv_cache.shape[1]
    local_heads = diff_lambda.shape[0]
    resid = residual_in.astype(jnp.float32)
    normed = rms_rows(resid, norm_gain_attn).astype(jnp.bfloat16)
    positions = lengths.astype(jnp.float32)
    query = jnp.dot(normed, query_weight, preferred_element_type=jnp.float32).reshape(
        seq_count, local_heads, 2, QK_DIM
    )
    query = rotate(query, positions).astype(jnp.bfloat16)
    keys = jnp.dot(normed, key_weight, preferred_element_type=jnp.float32).reshape(
        seq_count, groups, 2, QK_DIM
    )
    keys = rotate(keys, positions).astype(jnp.bfloat16).reshape(seq_count, groups, 2 * QK_DIM)
    values = (
        jnp.dot(normed, value_weight, preferred_element_type=jnp.float32)
        .reshape(seq_count, groups, HEAD_DIM)
        .astype(jnp.bfloat16)
    )
    fresh = jnp.concatenate([keys, values], axis=-1)
    mixed = attend(query, fresh, kv_cache, lengths, diff_lambda)
    heads_out = (
        rms_rows(mixed, head_gain).astype(jnp.bfloat16).reshape(seq_count, local_heads * HEAD_DIM)
    )
    all_heads = gather_directly(heads_out, "tp", 1)
    attn_cols = jnp.dot(all_heads, out_weight, preferred_element_type=jnp.float32)
    own_cols = lax.dynamic_slice_in_dim(resid, column * quarter, quarter, 1)
    stream_cols = (own_cols + attn_cols).astype(jnp.bfloat16)
    stream = gather_directly(stream_cols, "tp", 1)
    ffn_in = rms_rows(stream.astype(jnp.float32), norm_gain_ffn).astype(jnp.bfloat16)
    held = expert_gate.shape[0]
    expert_total = lax.axis_size("ep") * held
    capacity = max(2, 2 * TOPK * seq_count // expert_total)
    flat_ids = route_ids.reshape(-1)
    member = (flat_ids[:, None] == jnp.arange(expert_total, dtype=jnp.int32)[None, :]).astype(
        jnp.int32
    )
    slot = jnp.sum((jnp.cumsum(member, axis=0) - member) * member, axis=1)
    target = (flat_ids * capacity + slot).reshape(seq_count, TOPK)
    picker = (
        target[None, :, :] == jnp.arange(expert_total * capacity, dtype=jnp.int32)[:, None, None]
    )
    picker = jnp.any(picker, axis=2).astype(jnp.bfloat16)
    outgoing = jnp.dot(picker, ffn_in, preferred_element_type=jnp.float32).astype(jnp.bfloat16)
    outgoing = outgoing.reshape(expert_total, capacity, ffn_in.shape[1])
    arrived = lax.all_to_all(outgoing, "ep", split_axis=0, concat_axis=0, tiled=True)
    senders = arrived.shape[0] // held
    blocked = arrived.reshape(senders, held, arrived.shape[1], width)
    gate = jnp.einsum("sjcd,jdf->sjcf", blocked, expert_gate, preferred_element_type=jnp.float32)
    upward = jnp.einsum("sjcd,jdf->sjcf", blocked, expert_up, preferred_element_type=jnp.float32)
    hidden = (jax.nn.silu(gate) * upward).astype(jnp.bfloat16)
    partial_out = jnp.einsum(
        "sjcf,jfd->sjcd", hidden, expert_down, preferred_element_type=jnp.float32
    )
    partial_out = partial_out.reshape(arrived.shape[0], arrived.shape[1], width)
    summed = summed_on_arrival(partial_out.astype(jnp.bfloat16), "tp", 2)
    returned = lax.all_to_all(
        summed.astype(jnp.bfloat16), "ep", split_axis=0, concat_axis=0, tiled=True
    )
    flat_back = returned.reshape(expert_total * capacity, quarter)
    picked = flat_back[target]
    expert_cols = jnp.sum(route_weights[..., None] * picked.astype(jnp.float32), axis=1)
    gate_mix = jax.nn.sigmoid(jnp.sum(ffn_in.astype(jnp.float32) * dense_mix, axis=-1))
    piece = lax.all_gather(ffn_in, "ep", axis=0, tiled=True)
    gate = jnp.dot(piece, dense_gate, preferred_element_type=jnp.float32)
    upward = jnp.dot(piece, dense_up, preferred_element_type=jnp.float32)
    dense_hidden = (jax.nn.silu(gate) * upward).astype(jnp.bfloat16)
    down_part = lax.dynamic_slice_in_dim(dense_down, column * quarter, quarter, 1)
    dense_cols = summed_on_arrival(
        jnp.dot(dense_hidden, down_part, preferred_element_type=jnp.float32).astype(jnp.bfloat16),
        "ep",
        0,
    )
    layer_out = (
        stream_cols.astype(jnp.float32) + expert_cols + gate_mix[:, None] * dense_cols
    ).astype(jnp.bfloat16)
    return (layer_out, fresh)


def solution(mesh):
    placed = (
        P("ep", None),
        P("ep"),
        P("ep", "tp", None, None),
        P(),
        P(None, "tp"),
        P(None, "tp"),
        P(None, "tp"),
        P("tp"),
        P(),
        P(None, "tp"),
        P(),
        P("ep", None),
        P("ep", None),
        P("ep", None, "tp"),
        P("ep", None, "tp"),
        P("ep", "tp", None),
        P(None, "ep"),
        P(None, "ep"),
        P("ep", None),
        P(),
    )
    return jax.shard_map(
        on_device,
        mesh=mesh,
        in_specs=placed,
        out_specs=(P("ep", "tp"), P("ep", "tp", None)),
        check_vma=False,
    )
```

profile of v0, /device:TPU:1, one launch (start us, length us, event | category | flops | bytes accessed | tf_op | source)
XLA Modules:
  0.0 177.4 jit_solution(7542298937267518820)
XLA Ops:
  7.2 0.8 convert_element_type.131
  8.0 0.7 iota_compare_fusion
  8.7 1.0 multiply_reduce_fusion.1
  9.7 0.7 broadcast_bitcast_fusion
  10.4 1.3 fusion.73
  11.8 1.3 fusion.76
  13.6 1.3 fusion.74
  15.4 2.5 %fusion.12 = f32[16,4,512]{2,1,0:T(4,128)S(1)} fusion(bf16[16,4,64]{2,1,0:T(4,128)(2,1)S(1)} %get-tuple-element.10, bf16[16,1,512,256]{3,2,1,0:T(8,128)(2,1)} %param.22), kind=kOutput, calls=%fused_computation.17 | convolution fusion | flops 4227072 | bytes 2236416 | tf_op jit(solution)/shard_map/bgjd,bgkd->bgjk/dot_general | solution.py:83
  18.1 2.3 %select_reduce_fusion.1 = (f32[16,4]{1,0:T(8,128)S(1)}, f32[16,4]{1,0:T(8,128)S(1)}, f32[16,4,512]{2,1,0:T(4,128)S(1)}) fusion(pred[16,512]{1,0:T(8,128)(4,1)S(1)} %iota_compare_fusion, f32[16,4,512]{2,1,0:T(4,128)S(1)} %fusion.12, bf16[16,4,64]{2,1,0:T(4,128)(2,1)S(1)} %get-tuple-element.11, bf16[16,1,512,256]{3,2,1,0:T(8,128)(2,1)} %param.22), kind=kOutput, calls=%fused_computation.52 | convolution fusion | flops 4358016 | bytes 2376192 | tf_op jit(solution)/shard_map/bgjd,bgkd->bgjk/dot_general | solution.py:74
  20.8 0.6 multiply_reduce_fusion.3
  21.5 0.6 broadcast_in_dim.69
  22.1 5.0 %all-to-all-start = ((bf16[4,16,512]{2,1,0:T(8,128)(2,1)}), bf16[4,16,512]{2,1,0:T(8,128)(2,1)S(1)}, u32[]{:S(2)}, u32[]{:S(2)}) async-start(bf16[4,16,512]{2,1,0:T(8,128)(2,1)} %broadcast_in_dim.69), calls=%async_computation | async-start | bytes 131072 | tf_op jit(solution)/shard_map/all_to_all | solution.py:14
  27.1 4.5 %all-to-all-done = bf16[4,16,512]{2,1,0:T(8,128)(2,1)S(1)} async-done(((bf16[4,16,512]{2,1,0:T(8,128)(2,1)}), bf16[4,16,512]{2,1,0:T(8,128)(2,1)S(1)}, u32[]{:S(2)}, u32[]{:S(2)}) %all-to-all-start) | async-done | bytes 65568 | tf_op jit(solution)/shard_map/all_to_all | solution.py:14
  31.6 2.0 %fusion.19 = bf16[16,512]{1,0:T(8,128)(2,1)S(1)} fusion(bf16[16,2048]{1,0:T(8,128)(2,1)S(1)} %bitcast.127, bf16[2048,512]{1,0:T(8,128)(2,1)} %param.29, f32[16,2048]{1,0:T(8,128)S(1)} %convert_element_type.129, s32[]{:T(128)S(6)} %select_n.32), kind=kOutput, calls=%fused_computation.25 | convolution fusion | flops 33570816 | bytes 2211844 | tf_op jit(solution)/shard_map/dot_general | solution.py:177
  33.6 6.8 %all_to_all.30 = bf16[4,16,512]{2,1,0:T(8,128)(2,1)S(1)} all-to-all(bf16[4,16,512]{2,1,0:T(8,128)(2,1)S(1)} %broadcast_in_dim.70), channel_id=1, replica_groups=mesh['ep'=64,'tp'=4] {'tp'}, dimensions={0} | all-to-all | bytes 131072 | tf_op jit(solution)/shard_map/all_to_all | solution.py:14
  40.6 0.7 multiply_convert_fusion
  42.1 1.2 convolution_convert_fusion.1
  43.7 33.7 %all_to_all.31 = bf16[64,2,2048]{2,1,0:T(2,128)(2,1)S(1)} all-to-all(bf16[64,2,2048]{2,1,0:T(2,128)(2,1)S(1)} %reshape.369), channel_id=1, replica_groups=mesh['ep'=64,'tp'=4] {'ep'}, dimensions={0} | all-to-all | bytes 1048576 | tf_op jit(solution)/shard_map/all_to_all | solution.py:197
  77.3 1.4 convolution_bitcast_fusion.1
  78.7 1.8 %fusion = bf16[64,1,2,2048]{3,0,2,1:T(8,128)(2,1)S(1)} fusion(bf16[1,128,2048]{2,1,0:T(8,128)(2,1)} %param.35, bf16[1,2048,128]{2,1,0:T(8,128)(2,1)} %param.34, bf16[64,2,2048]{2,1,0:T(2,128)(2,1)S(1)} %all_to_all.31, f32[64,1,2,128]{3,0,2,1:T(8,128)S(1)} %convolution_bitcast_fusion.1), kind=kOutput, calls=%fused_computation.3 | convolution fusion | flops 134578176 | bytes 2162688 | tf_op jit(solution)/shard_map/sjcf,jfd->sjcd/dot_general | solution.py:203
  80.5 0.4 convert_element_type.153
  81.0 11.8 %all_to_all.32 = bf16[4,64,2,512]{3,1,2,0:T(8,128)(2,1)S(1)} all-to-all(bf16[4,64,2,512]{3,1,2,0:T(8,128)(2,1)S(1)} %bitcast.123), channel_id=1, replica_groups=mesh['ep'=64,'tp'=4] {'tp'}, dimensions={0} | all-to-all | bytes 1048576 | tf_op jit(solution)/shard_map/all_to_all | solution.py:36
  92.9 0.8 copy.105
  93.6 6.3 %all-to-all-start.4 = ((bf16[64,2,512]{2,1,0:T(2,128)(2,1)}), bf16[64,2,512]{2,1,0:T(2,128)(2,1)S(1)}, u32[]{:S(2)}, u32[]{:S(2)}) async-start(bf16[64,2,512]{2,1,0:T(2,128)(2,1)} %copy.105), calls=%async_computation.4 | async-start | bytes 262144 | tf_op jit(solution)/shard_map/all_to_all | solution.py:208
  99.9 26.2 %all-gather.2.cloned.1.call-done = bf16[1024,2048]{1,0:T(8,128)(2,1)} async-done(((bf16[16,2048]{1,0:T(8,128)(2,1)}), bf16[1024,2048]{1,0:T(8,128)(2,1)}) %all-gather.2.cloned.1.call-update) | async-done | bytes 4194320 | tf_op jit(solution)/shard_map/all_gather | solution.py:215
  126.1 3.4 %fusion.77 = f32[1024,128]{1,0:T(8,128)S(1)} fusion(bf16[1024,2048]{1,0:T(8,128)(2,1)} %all-gather.2.cloned.1.call-done, bf16[2048,128]{1,0:T(8,128)(2,1)S(1)} %copy-done.3), kind=kOutput, calls=%fused_computation.130 | convolution fusion | flops 536870912 | bytes 5242880 | tf_op jit(solution)/shard_map/dot_general | solution.py:216
  129.6 5.3 %convolution_convert_fusion.2 = bf16[1024,512]{1,0:T(8,128)(2,1)} fusion(bf16[1024,2048]{1,0:T(8,128)(2,1)} %all-gather.2.cloned.1.call-done, bf16[2048,128]{1,0:T(8,128)(2,1)} %param.37, f32[1024,128]{1,0:T(8,128)S(1)} %fusion.77, bf16[128,2048]{1,0:T(8,128)(2,1)} %param.38, s32[]{:T(128)S(6)} %select_n.32), kind=kOutput, calls=%fused_computation.13 | convolution fusion | flops 672399360 | bytes 6422532 | tf_op jit(solution)/shard_map/dot_general | solution.py:221
  134.8 6.7 %all-to-all-start.5 = ((bf16[64,16,512]{2,1,0:T(8,128)(2,1)}), bf16[64,16,512]{2,1,0:T(8,128)(2,1)S(1)}, u32[]{:S(2)}, u32[]{:S(2)}) async-start(bf16[64,16,512]{2,1,0:T(8,128)(2,1)} %bitcast.125), calls=%async_computation.5 | async-start | bytes 2097152 | tf_op jit(solution)/shard_map/all_to_all | solution.py:36
  141.8 0.6 pad_maximum_fusion.2
  142.7 0.6 gather_fusion
  143.6 26.1 %all-to-all-done.5 = bf16[64,16,512]{2,1,0:T(8,128)(2,1)S(1)} async-done(((bf16[64,16,512]{2,1,0:T(8,128)(2,1)}), bf16[64,16,512]{2,1,0:T(8,128)(2,1)S(1)}, u32[]{:S(2)}, u32[]{:S(2)}) %all-to-all-start.5) | async-done | bytes 1048608 | tf_op jit(solution)/shard_map/all_to_all | solution.py:36
  169.9 0.7 add_convert_fusion.1
  (72 shorter events, 4.1 us)
Async XLA Ops:
  7.2 6.4 %copy-start = (bf16[2048,512]{1,0:T(8,128)(2,1)S(1)}, bf16[2048,512]{1,0:T(8,128)(2,1)}, u32[]{:S(2)}) copy-start(bf16[2048,512]{1,0:T(8,128)(2,1)} %param.24) | copy-start | bytes 6291460
  15.4 5.3 %copy-start.8 = (f32[4]{0:T(128)S(1)}, f32[4]{0:T(128)}, u32[]{:S(2)}) copy-start(f32[4]{0:T(128)} %param.27) | copy-start | bytes 52
  15.4 5.3 %copy-start.2 = (bf16[16,1,512,256]{3,2,1,0:T(8,128)(2,1)S(1)}, bf16[16,1,512,256]{3,2,1,0:T(8,128)(2,1)}, u32[]{:S(2)}) copy-start(bf16[16,1,512,256]{3,2,1,0:T(8,128)(2,1)} %param.22) | copy-start | bytes 12582916
  20.8 6.4 %copy-start.1 = (bf16[16,2048]{1,0:T(8,128)(2,1)S(1)}, bf16[16,2048]{1,0:T(8,128)(2,1)}, u32[]{:S(2)}) copy-start(bf16[16,2048]{1,0:T(8,128)(2,1)} %param.20) | copy-start | bytes 196612
  21.4 19.2 %copy-start.4 = (f32[2048]{0:T(1024)S(1)}, f32[2048]{0:T(1024)}, u32[]{:S(2)}) copy-start(f32[2048]{0:T(1024)} %param.30) | copy-start | bytes 24580
  21.4 20.0 %copy-start.6 = (s32[16,2]{0,1:T(2,128)S(1)}, s32[16,2]{0,1:T(2,128)}, u32[]{:S(2)}) copy-start(s32[16,2]{0,1:T(2,128)} %param.31) | copy-start | bytes 388
  22.1 9.5 %all-to-all-start = ((bf16[4,16,512]{2,1,0:T(8,128)(2,1)}), bf16[4,16,512]{2,1,0:T(8,128)(2,1)S(1)}, u32[]{:S(2)}, u32[]{:S(2)}) async-start(bf16[4,16,512]{2,1,0:T(8,128)(2,1)} %broadcast_in_dim.69), calls=%async_computation | async-start | bytes 131072 | tf_op jit(solution)/shard_map/all_to_all | solution.py:14
  27.1 99.0 %all-gather.2.cloned.1.call-start = ((), (), s32[]{:S(2)}) async-start(), calls=%async_computation.6 | async-start | bytes 4259840 | tf_op jit(solution)/shard_map/all_gather | solution.py:215
  80.9 45.2 %copy-start.3 = (bf16[2048,128]{1,0:T(8,128)(2,1)S(1)}, bf16[2048,128]{1,0:T(8,128)(2,1)}, u32[]{:S(2)}) copy-start(bf16[2048,128]{1,0:T(8,128)(2,1)} %param.36) | copy-start | bytes 1572868
  93.6 41.2 %all-to-all-start.4 = ((bf16[64,2,512]{2,1,0:T(2,128)(2,1)}), bf16[64,2,512]{2,1,0:T(2,128)(2,1)S(1)}, u32[]{:S(2)}, u32[]{:S(2)}) async-start(bf16[64,2,512]{2,1,0:T(2,128)(2,1)} %copy.105), calls=%async_computation.4 | async-start | bytes 262144 | tf_op jit(solution)/shard_map/all_to_all | solution.py:208
  134.8 6.7 %copy-start.7 = (f32[16,2]{0,1:T(2,128)S(1)}, f32[16,2]{0,1:T(2,128)}, u32[]{:S(2)}) copy-start(f32[16,2]{0,1:T(2,128)} %param.32) | copy-start | bytes 388
  134.8 6.8 %copy-start.5 = (f32[2048]{0:T(1024)S(1)}, f32[2048]{0:T(1024)}, u32[]{:S(2)}) copy-start(f32[2048]{0:T(1024)} %param.39) | copy-start | bytes 24580
  134.8 34.9 %all-to-all-start.5 = ((bf16[64,16,512]{2,1,0:T(8,128)(2,1)}), bf16[64,16,512]{2,1,0:T(8,128)(2,1)S(1)}, u32[]{:S(2)}, u32[]{:S(2)}) async-start(bf16[64,16,512]{2,1,0:T(8,128)(2,1)} %bitcast.125), calls=%async_computation.5 | async-start | bytes 2097152 | tf_op jit(solution)/shard_map/all_to_all | solution.py:36
Sparse Core Ops, SparseCore 0:
  41.5 84.6 all-gather.1
where the time goes:
time: 178 us; the launch traced here: 177 us
  waiting for transfers between devices  56.8 us (32%)
  blocking collectives  52.3 us (29%)
  matrix products  24.6 us (14%)
  starting transfers between devices  18 us (10%)
  between operations  14.3 us (8%)
  other arithmetic  6.57 us (4%)
  local copies, waits for them, and re-layouts  4.77 us (3%)
    all_to_all x1, blocking collectives, on_device(): lax.all_to_all(outgoing, 'ep', split_axis=0, concat_axis=0, tiled=True)  33.7 us
    all_gather x1, waiting for transfers between devices, on_device(): piece = lax.all_gather(ffn_in, 'ep', axis=0, tiled=True)  26.2 us
    all_to_all x1, waiting for transfers between devices, summed_on_arrival(): lax.all_to_all(pieces, axis, split_axis=0, concat_axis=0, tiled=True)  26.1 us
    all_to_all x1, blocking collectives, summed_on_arrival(): lax.all_to_all(pieces, axis, split_axis=0, concat_axis=0, tiled=True)  11.8 us
    all_to_all x1, blocking collectives, from_everyone(): return lax.all_to_all(copies, axis, split_axis=0, concat_axis=0, tiled=True)  6.84 us
    all_to_all x1, starting transfers between devices, summed_on_arrival(): lax.all_to_all(pieces, axis, split_axis=0, concat_axis=0, tiled=True)  6.69 us
    all_to_all x1, starting transfers between devices, on_device(): lax.all_to_all(summed.astype(jnp.bfloat16), 'ep', split_axis=0, concat_ax...  6.29 us
    dot_general x1, matrix products, on_device(): jnp.dot(dense_hidden, down_part, preferred_element_type=jnp.float32)  5.25 us
  transfers between devices with their start and end apart: 4, of which 3 were waited for; matrix products, arithmetic and copies ran while one was open for 10% of the time, Pallas kernels for 0%

commit v1 on v0

--- a/solution.py
+++ b/solution.py
@@ -212,7 +212,8 @@
     picked = flat_back[target]
     expert_cols = jnp.sum(route_weights[..., None] * picked.astype(jnp.float32), axis=1)
     gate_mix = jax.nn.sigmoid(jnp.sum(ffn_in.astype(jnp.float32) * dense_mix, axis=-1))
-    piece = lax.all_gather(ffn_in, "ep", axis=0, tiled=True)
+    copies_2 = jnp.concatenate([ffn_in] * lax.axis_size("ep"), axis=0)
+    piece = lax.all_to_all(copies_2, "ep", 0, 0, tiled=True)
     gate = jnp.dot(piece, dense_gate, preferred_element_type=jnp.float32)
     upward = jnp.dot(piece, dense_up, preferred_element_type=jnp.float32)
     dense_hidden = (jax.nn.silu(gate) * upward).astype(jnp.bfloat16)

time: 178 us -> 278 us (1.56)
  waiting for transfers between devices: 56.8 us -> 153 us
  blocking collectives: 52.3 us -> 0 us
  local copies, waits for them, and re-layouts: 4.77 us -> 46.2 us
  starting transfers between devices: 18 us -> 47.7 us
  between operations: 14.3 us -> 1.02 us
    all_to_all x0 -> x2, waiting for transfers between devices: none -> 108 us  [the longest x1 93.9 us: on_device(): piece = lax.all_to_all(copies_2, 'ep', 0, 0, tiled=True)]
    all_to_all x3 -> x0, blocking collectives: 52.3 us -> none  [the longest x1 33.7 us: on_device(): lax.all_to_all(outgoing, 'ep', split_axis=0, concat_axis=0, tiled=True)]
    unnamed x20 -> x84, local copies, waits for them, and re-layouts: 0.21 us -> 38.7 us
    all_gather x1 -> x0, waiting for transfers between devices: 26.2 us -> none  [on_device(): piece = lax.all_gather(ffn_in, 'ep', axis=0, tiled=True)]
    all_to_all x0 -> x2, starting transfers between devices: none -> 21.2 us  [the longest x1 14.7 us: on_device(): lax.all_to_all(outgoing, 'ep', split_axis=0, concat_axis=0, tiled=True)]
    all_to_all x1 -> x2, waiting for transfers between devices: 26.1 us -> 34 us  [summed_on_arrival(): lax.all_to_all(pieces, axis, split_axis=0, concat_axis=0, tiled=True)]
    all_to_all x1 -> x2, starting transfers between devices: 6.69 us -> 11.4 us  [summed_on_arrival(): lax.all_to_all(pieces, axis, split_axis=0, concat_axis=0, tiled=True)]
    all_to_all x1 -> x2, waiting for transfers between devices: 4.45 us -> 8.13 us  [from_everyone(): return lax.all_to_all(copies, axis, split_axis=0, concat_axis=0, tiled=True)]
  transfers between devices with their start and end apart: 4 -> 7, of which waited for: 3 -> 7; matrix products, arithmetic and copies ran while one was open for 10% -> 6% of each run, Pallas kernels for 0% -> 0%
where the time goes in v1:
time: 278 us; the launch traced here: 277 us
  waiting for transfers between devices  153 us (55%)
  starting transfers between devices  47.7 us (17%)
  local copies, waits for them, and re-layouts  46.2 us (17%)
  matrix products  22.8 us (8%)
  other arithmetic  6.58 us (2%)
    all_to_all x1, waiting for transfers between devices, on_device(): piece = lax.all_to_all(copies_2, 'ep', 0, 0, tiled=True)  93.9 us
    unnamed x84, local copies, waits for them, and re-layouts  38.7 us
    all_to_all x2, waiting for transfers between devices, summed_on_arrival(): lax.all_to_all(pieces, axis, split_axis=0, concat_axis=0, tiled=True)  34 us
    all_to_all x1, starting transfers between devices, on_device(): lax.all_to_all(outgoing, 'ep', split_axis=0, concat_axis=0, tiled=True)  14.7 us
    all_to_all x1, waiting for transfers between devices, on_device(): lax.all_to_all(outgoing, 'ep', split_axis=0, concat_axis=0, tiled=True)  14.6 us
    all_to_all x2, starting transfers between devices, summed_on_arrival(): lax.all_to_all(pieces, axis, split_axis=0, concat_axis=0, tiled=True)  11.4 us
    all_to_all x2, starting transfers between devices, from_everyone(): return lax.all_to_all(copies, axis, split_axis=0, concat_axis=0, tiled=True)  8.28 us
    all_to_all x2, waiting for transfers between devices, from_everyone(): return lax.all_to_all(copies, axis, split_axis=0, concat_axis=0, tiled=True)  8.13 us
  transfers between devices with their start and end apart: 7, of which 7 were waited for; matrix products, arithmetic and copies ran while one was open for 6% of the time, Pallas kernels for 0%

profile of v1, /device:TPU:1, one launch (start us, length us, event | category | flops | bytes accessed | tf_op | source)
XLA Modules:
  0.0 277.3 jit_solution(9673626823140413173)
XLA Ops:
  0.7 0.8 convert_element_type.131
  1.5 0.7 iota_compare_fusion
  2.2 1.0 multiply_reduce_fusion.1
  3.2 0.7 broadcast_bitcast_fusion
  3.8 1.3 fusion.73
  5.2 1.3 fusion.76
  7.1 1.3 fusion.74
  8.9 2.6 fusion.12
  11.6 2.3 select_reduce_fusion.1
  15.7 5.0 %all-to-all-start = ((bf16[4,16,512]{2,1,0:T(8,128)(2,1)}), bf16[4,16,512]{2,1,0:T(8,128)(2,1)S(1)}, u32[]{:S(2)}, u32[]{:S(2)}) async-start(bf16[4,16,512]{2,1,0:T(8,128)(2,1)} %broadcast_in_dim.69), calls=%async_computation | async-start | bytes 131072 | tf_op jit(solution)/shard_map/all_to_all | solution.py:14
  21.4 3.8 %all-to-all-done = bf16[4,16,512]{2,1,0:T(8,128)(2,1)S(1)} async-done(((bf16[4,16,512]{2,1,0:T(8,128)(2,1)}), bf16[4,16,512]{2,1,0:T(8,128)(2,1)S(1)}, u32[]{:S(2)}, u32[]{:S(2)}) %all-to-all-start) | async-done | bytes 65568 | tf_op jit(solution)/shard_map/all_to_all | solution.py:14
  25.1 2.0 fusion.19
  27.8 3.3 %all-to-all-start.1 = ((bf16[4,16,512]{2,1,0:T(8,128)(2,1)}), bf16[4,16,512]{2,1,0:T(8,128)(2,1)S(1)}, u32[]{:S(2)}, u32[]{:S(2)}) async-start(bf16[4,16,512]{2,1,0:T(8,128)(2,1)} %broadcast_in_dim.70), calls=%async_computation.1 | async-start | bytes 131072 | tf_op jit(solution)/shard_map/all_to_all | solution.py:14
  31.1 4.4 %all-to-all-done.1 = bf16[4,16,512]{2,1,0:T(8,128)(2,1)S(1)} async-done(((bf16[4,16,512]{2,1,0:T(8,128)(2,1)}), bf16[4,16,512]{2,1,0:T(8,128)(2,1)S(1)}, u32[]{:S(2)}, u32[]{:S(2)}) %all-to-all-start.1) | async-done | bytes 65568 | tf_op jit(solution)/shard_map/all_to_all | solution.py:14
  35.7 0.7 constant_dynamic-update-slice_fusion.63
  71.6 1.1 reshape.371
  72.7 14.7 %all-to-all-start.2 = ((bf16[64,2,2048]{2,1,0:T(2,128)(2,1)}), bf16[64,2,2048]{2,1,0:T(2,128)(2,1)S(1)}, u32[]{:S(2)}, u32[]{:S(2)}) async-start(bf16[64,2,2048]{2,1,0:T(2,128)(2,1)} %reshape.371), calls=%async_computation.2 | async-start | bytes 1048576 | tf_op jit(solution)/shard_map/all_to_all | solution.py:197
  90.5 14.6 %all-to-all-done.2 = bf16[64,2,2048]{2,1,0:T(2,128)(2,1)S(1)} async-done(((bf16[64,2,2048]{2,1,0:T(2,128)(2,1)}), bf16[64,2,2048]{2,1,0:T(2,128)(2,1)S(1)}, u32[]{:S(2)}, u32[]{:S(2)}) %all-to-all-start.2) | async-done | bytes 524320 | tf_op jit(solution)/shard_map/all_to_all | solution.py:197
  105.5 1.8 fusion
  107.7 0.9 copy.142
  108.5 3.5 %all-to-all-start.3 = ((bf16[4,64,2,512]{3,1,2,0:T(8,128)(2,1)}), bf16[4,64,2,512]{3,1,2,0:T(8,128)(2,1)S(1)}, u32[]{:S(2)}, u32[]{:S(2)}) async-start(bf16[4,64,2,512]{3,1,2,0:T(8,128)(2,1)} %bitcast.124), calls=%async_computation.3 | async-start | bytes 1048576 | tf_op jit(solution)/shard_map/all_to_all | solution.py:36
  113.3 7.9 %all-to-all-done.3 = bf16[4,64,2,512]{3,1,2,0:T(8,128)(2,1)S(1)} async-done(((bf16[4,64,2,512]{3,1,2,0:T(8,128)(2,1)}), bf16[4,64,2,512]{3,1,2,0:T(8,128)(2,1)S(1)}, u32[]{:S(2)}, u32[]{:S(2)}) %all-to-all-start.3) | async-done | bytes 524320 | tf_op jit(solution)/shard_map/all_to_all | solution.py:36
  121.2 6.5 %all-to-all-start.5 = ((bf16[64,16,2048]{2,1,0:T(8,128)(2,1)}), bf16[64,16,2048]{2,1,0:T(8,128)(2,1)}, u32[]{:S(2)}, u32[]{:S(2)}) async-start(bf16[64,16,2048]{2,1,0:T(8,128)(2,1)} %bitcast.38), calls=%async_computation.5 | async-start | bytes 8388608 | tf_op jit(solution)/shard_map/all_to_all | solution.py:216
  127.8 0.8 copy.105
  128.6 93.9 %all-to-all-done.5 = bf16[64,16,2048]{2,1,0:T(8,128)(2,1)} async-done(((bf16[64,16,2048]{2,1,0:T(8,128)(2,1)}), bf16[64,16,2048]{2,1,0:T(8,128)(2,1)}, u32[]{:S(2)}, u32[]{:S(2)}) %all-to-all-start.5) | async-done | bytes 4194336 | tf_op jit(solution)/shard_map/all_to_all | solution.py:216
  222.4 6.8 %all-to-all-start.4 = ((bf16[64,2,512]{2,1,0:T(2,128)(2,1)}), bf16[64,2,512]{2,1,0:T(2,128)(2,1)S(1)}, u32[]{:S(2)}, u32[]{:S(2)}) async-start(bf16[64,2,512]{2,1,0:T(2,128)(2,1)} %copy.105), calls=%async_computation.4 | async-start | bytes 262144 | tf_op jit(solution)/shard_map/all_to_all | solution.py:208
  229.2 3.4 %fusion.77 = f32[1024,128]{1,0:T(8,128)S(1)} fusion(bf16[1024,2048]{1,0:T(8,128)(2,1)} %bitcast.39, bf16[2048,128]{1,0:T(8,128)(2,1)S(1)} %copy-done.3), kind=kOutput, calls=%fused_computation.194 | convolution fusion | flops 536870912 | bytes 5242880 | tf_op jit(solution)/shard_map/dot_general | solution.py:217
  232.7 5.3 %convolution_convert_fusion.2 = bf16[1024,512]{1,0:T(8,128)(2,1)} fusion(bf16[1024,2048]{1,0:T(8,128)(2,1)} %bitcast.39, bf16[2048,128]{1,0:T(8,128)(2,1)} %param.37, f32[1024,128]{1,0:T(8,128)S(1)} %fusion.77, bf16[128,2048]{1,0:T(8,128)(2,1)} %param.38, s32[]{:T(128)S(6)} %select_n.32), kind=kOutput, calls=%fused_computation.13 | convolution fusion | flops 672399360 | bytes 6422532 | tf_op jit(solution)/shard_map/dot_general | solution.py:222
  238.0 2.4 all-to-all-done.4
  240.3 7.9 %all-to-all-start.6 = ((bf16[64,16,512]{2,1,0:T(8,128)(2,1)}), bf16[64,16,512]{2,1,0:T(8,128)(2,1)S(1)}, u32[]{:S(2)}, u32[]{:S(2)}) async-start(bf16[64,16,512]{2,1,0:T(8,128)(2,1)} %bitcast.126), calls=%async_computation.6 | async-start | bytes 2097152 | tf_op jit(solution)/shard_map/all_to_all | solution.py:36
  250.3 26.1 %all-to-all-done.6 = bf16[64,16,512]{2,1,0:T(8,128)(2,1)S(1)} async-done(((bf16[64,16,512]{2,1,0:T(8,128)(2,1)}), bf16[64,16,512]{2,1,0:T(8,128)(2,1)S(1)}, u32[]{:S(2)}, u32[]{:S(2)}) %all-to-all-start.6) | async-done | bytes 1048608 | tf_op jit(solution)/shard_map/all_to_all | solution.py:36
  276.6 0.7 add_convert_fusion.1
  (139 shorter events, 46.9 us)
Async XLA Ops:
  0.6 6.4 %copy-start = (bf16[2048,512]{1,0:T(8,128)(2,1)S(1)}, bf16[2048,512]{1,0:T(8,128)(2,1)}, u32[]{:S(2)}) copy-start(bf16[2048,512]{1,0:T(8,128)(2,1)} %param.24) | copy-start | bytes 6291460
  6.6 7.7 %copy-start.9 = (f32[4]{0:T(128)S(1)}, f32[4]{0:T(128)}, u32[]{:S(2)}) copy-start(f32[4]{0:T(128)} %param.27) | copy-start | bytes 52
  8.5 5.9 %copy-start.2 = (bf16[16,1,512,256]{3,2,1,0:T(8,128)(2,1)S(1)}, bf16[16,1,512,256]{3,2,1,0:T(8,128)(2,1)}, u32[]{:S(2)}) copy-start(bf16[16,1,512,256]{3,2,1,0:T(8,128)(2,1)} %param.22) | copy-start | bytes 12582916
  11.5 9.2 %copy-start.7 = (s32[16,2]{0,1:T(2,128)S(1)}, s32[16,2]{0,1:T(2,128)}, u32[]{:S(2)}) copy-start(s32[16,2]{0,1:T(2,128)} %param.31) | copy-start | bytes 388
  11.5 9.9 %copy-start.1 = (bf16[16,2048]{1,0:T(8,128)(2,1)S(1)}, bf16[16,2048]{1,0:T(8,128)(2,1)}, u32[]{:S(2)}) copy-start(bf16[16,2048]{1,0:T(8,128)(2,1)} %param.20) | copy-start | bytes 196612
  14.3 21.3 %copy-start.5 = (f32[2048]{0:T(1024)S(1)}, f32[2048]{0:T(1024)}, u32[]{:S(2)}) copy-start(f32[2048]{0:T(1024)} %param.30) | copy-start | bytes 24580
  15.7 9.5 %all-to-all-start = ((bf16[4,16,512]{2,1,0:T(8,128)(2,1)}), bf16[4,16,512]{2,1,0:T(8,128)(2,1)S(1)}, u32[]{:S(2)}, u32[]{:S(2)}) async-start(bf16[4,16,512]{2,1,0:T(8,128)(2,1)} %broadcast_in_dim.69), calls=%async_computation | async-start | bytes 131072 | tf_op jit(solution)/shard_map/all_to_all | solution.py:14
  27.8 7.7 %all-to-all-start.1 = ((bf16[4,16,512]{2,1,0:T(8,128)(2,1)}), bf16[4,16,512]{2,1,0:T(8,128)(2,1)S(1)}, u32[]{:S(2)}, u32[]{:S(2)}) async-start(bf16[4,16,512]{2,1,0:T(8,128)(2,1)} %broadcast_in_dim.70), calls=%async_computation.1 | async-start | bytes 131072 | tf_op jit(solution)/shard_map/all_to_all | solution.py:14
  47.6 57.6 %copy-start.4 = (bf16[1,2048,128]{2,1,0:T(8,128)(2,1)S(1)}, bf16[1,2048,128]{2,1,0:T(8,128)(2,1)}, u32[]{:S(2)}) copy-start(bf16[1,2048,128]{2,1,0:T(8,128)(2,1)} %param.33) | copy-start | bytes 1572868
  72.7 32.4 %all-to-all-start.2 = ((bf16[64,2,2048]{2,1,0:T(2,128)(2,1)}), bf16[64,2,2048]{2,1,0:T(2,128)(2,1)S(1)}, u32[]{:S(2)}, u32[]{:S(2)}) async-start(bf16[64,2,2048]{2,1,0:T(2,128)(2,1)} %reshape.371), calls=%async_computation.2 | async-start | bytes 1048576 | tf_op jit(solution)/shard_map/all_to_all | solution.py:197
  108.5 12.6 %all-to-all-start.3 = ((bf16[4,64,2,512]{3,1,2,0:T(8,128)(2,1)}), bf16[4,64,2,512]{3,1,2,0:T(8,128)(2,1)S(1)}, u32[]{:S(2)}, u32[]{:S(2)}) async-start(bf16[4,64,2,512]{3,1,2,0:T(8,128)(2,1)} %bitcast.124), calls=%async_computation.3 | async-start | bytes 1048576 | tf_op jit(solution)/shard_map/all_to_all | solution.py:36
  121.2 108.1 %copy-start.3 = (bf16[2048,128]{1,0:T(8,128)(2,1)S(1)}, bf16[2048,128]{1,0:T(8,128)(2,1)}, u32[]{:S(2)}) copy-start(bf16[2048,128]{1,0:T(8,128)(2,1)} %param.36) | copy-start | bytes 1572868
  121.2 101.2 %all-to-all-start.5 = ((bf16[64,16,2048]{2,1,0:T(8,128)(2,1)}), bf16[64,16,2048]{2,1,0:T(8,128)(2,1)}, u32[]{:S(2)}, u32[]{:S(2)}) async-start(bf16[64,16,2048]{2,1,0:T(8,128)(2,1)} %bitcast.38), calls=%async_computation.5 | async-start | bytes 8388608 | tf_op jit(solution)/shard_map/all_to_all | solution.py:216
  222.4 17.9 %all-to-all-start.4 = ((bf16[64,2,512]{2,1,0:T(2,128)(2,1)}), bf16[64,2,512]{2,1,0:T(2,128)(2,1)S(1)}, u32[]{:S(2)}, u32[]{:S(2)}) async-start(bf16[64,2,512]{2,1,0:T(2,128)(2,1)} %copy.105), calls=%async_computation.4 | async-start | bytes 262144 | tf_op jit(solution)/shard_map/all_to_all | solution.py:208
  232.7 15.6 %copy-start.8 = (f32[16,2]{0,1:T(2,128)S(1)}, f32[16,2]{0,1:T(2,128)}, u32[]{:S(2)}) copy-start(f32[16,2]{0,1:T(2,128)} %param.32) | copy-start | bytes 388
  232.7 15.7 %copy-start.6 = (f32[2048]{0:T(1024)S(1)}, f32[2048]{0:T(1024)}, u32[]{:S(2)}) copy-start(f32[2048]{0:T(1024)} %param.39) | copy-start | bytes 24580
  240.3 36.1 %all-to-all-start.6 = ((bf16[64,16,512]{2,1,0:T(8,128)(2,1)}), bf16[64,16,512]{2,1,0:T(8,128)(2,1)S(1)}, u32[]{:S(2)}, u32[]{:S(2)}) async-start(bf16[64,16,512]{2,1,0:T(8,128)(2,1)} %bitcast.126), calls=%async_computation.6 | async-start | bytes 2097152 | tf_op jit(solution)/shard_map/all_to_all | solution.py:36
